TPU v7x, 32 devices: a whole 2x2x4 slice. The times are simulated.
32 devices in a mesh: grp: 2 (over x), ep: 4 (over y, core), tp: 4 (over z).
Axes of the slice: x: 2, y: 2, z: 4, core: 2. Of those that a mesh axis runs over, the one named last changes fastest.
Arguments:
- tokens: bfloat16 [3072, 4096], P(('grp', 'ep'), 'tp'), parts along dimension 0
- pre_gain: float32 [4096], replicated, may hold values from 0.1 to 1.9
- out_gain: float32 [4096], P('tp'), may hold values from 0.1 to 1.9
- chosen: int32 [8, 4, 48], P(('grp', 'ep')), parts along dimension 0, may hold values from 0 to 383, as said below
- route_weight: float32 [8, 4, 48], P(('grp', 'ep')), parts along dimension 0, may hold values from 0.3 to 3
- expert_gate: bfloat16 [4, 4096, 3072], P('ep', None, 'tp'), may hold values from -0.09375 to 0.09375
- expert_up: bfloat16 [4, 4096, 3072], P('ep', None, 'tp'), may hold values from -0.09375 to 0.09375
- expert_down: bfloat16 [4, 3072, 4096], P('ep', 'tp'), may hold values from -0.109375 to 0.109375
Outputs:
- output: bfloat16 [3072, 4096], P(('grp', 'ep'), 'tp'), parts along dimension 0
There are 2 independent parts, one for each index of `grp`. A program takes and returns all parts, laid end to end along the dimension named above; an argument that names none is the same for every part. Nothing has to cross between parts.
Inputs may be any that keep to these rules, and one draw needn't show every extreme that they name: chosen[b, e, k] is the position, within block b of 384 tokens, of the k-th token that expert e takes from that block; the 48 positions of one block and one expert are all different.
All inputs are finite; a program needn't handle non-finite values.
Results may differ from a plain program's by a relative error of at most 0.0075.
Values may be sent and summed in bfloat16 or wider, within the bound.
No kernel may reach another device: no remote copies, remote signals or barrier semaphores. Data moves between devices by JAX's collectives and lax.ppermute only.
A program may use at most 64 MiB of HBM per device.

v0:
```python
import jax
import jax.numpy as jnp
from jax import lax
from jax.sharding import PartitionSpec as P

NORM_EPS = 1e-06


def shards(tokens, pre_gain, out_gain, chosen, route_weight, expert_gate, expert_up, expert_down):
    model_width = pre_gain.shape[0]
    shard_width = tokens.shape[1]
    tok_count = tokens.shape[0]
    chosen_here = chosen[0]
    experts_all = chosen_here.shape[0]
    slot_count = chosen_here.shape[1]
    resident = tokens.astype(jnp.float32)
    square_sum = lax.psum(jnp.sum(resident * resident, axis=1), "tp")
    row_scale = lax.rsqrt(square_sum / model_width + NORM_EPS)[:, None]
    gain_slice = lax.dynamic_slice_in_dim(
        pre_gain, lax.axis_index("tp") * shard_width, shard_width, 0
    )
    normed = (resident * row_scale * gain_slice).astype(jnp.bfloat16)
    outgoing = jnp.take(normed, chosen_here, axis=0)
    incoming = lax.all_to_all(outgoing, "ep", split_axis=0, concat_axis=0, tiled=True)
    picked_rows = lax.all_gather(incoming.reshape(-1, shard_width), "tp", axis=1, tiled=True)
    gate_act = jnp.dot(picked_rows, expert_gate[0], preferred_element_type=jnp.float32)
    up_act = jnp.dot(picked_rows, expert_up[0], preferred_element_type=jnp.float32)
    hidden = (jax.nn.silu(gate_act) * up_act).astype(jnp.bfloat16)
    down_shard = expert_down[0]
    summed = lax.psum_scatter(
        lax.dot_general(
            down_shard, hidden, (((0,), (1,)), ((), ())), preferred_element_type=jnp.float32
        ).astype(jnp.bfloat16),
        "tp",
        scatter_dimension=0,
        tiled=True,
    )
    expert_out = summed.reshape(shard_width, experts_all, slot_count)
    returned = lax.all_to_all(expert_out, "ep", split_axis=1, concat_axis=1, tiled=True)
    weighted = returned.astype(jnp.float32) * route_weight[0][None]
    flat_weighted = weighted.reshape(shard_width, experts_all * slot_count)
    update_cols = (
        jnp.zeros((shard_width, tok_count), jnp.float32)
        .at[:, chosen_here.reshape(-1)]
        .add(flat_weighted)
    )
    mixed_rows = resident + update_cols.T
    out_sum = lax.psum(jnp.sum(mixed_rows * mixed_rows, axis=1), "tp")
    out_scale = lax.rsqrt(out_sum / model_width + NORM_EPS)[:, None]
    return (mixed_rows * out_scale * out_gain).astype(jnp.bfloat16)


def solution(mesh):
    return jax.shard_map(
        shards,
        mesh=mesh,
        in_specs=(
            P(("grp", "ep"), "tp"),
            P(),
            P("tp"),
            P(("grp", "ep"), None, None),
            P(("grp", "ep"), None, None),
            P("ep", None, "tp"),
            P("ep", None, "tp"),
            P("ep", "tp", None),
        ),
        out_specs=P(("grp", "ep"), "tp"),
        check_vma=False,
    )
```

profile of v0, /device:TPU:0, one launch (start us, length us, event | category | flops | bytes accessed | tf_op | source)
XLA Modules:
  0.0 150.9 jit_solution(1247583569600255627)
XLA Ops:
  6.5 0.7 compare_select_fusion.1
  7.2 0.7 compare_and_fusion
  7.9 1.4 fusion.12
  9.3 13.5 %psum.14 = f32[384]{0:T(512)S(1)} all-reduce(f32[384]{0:T(512)S(1)} %fusion.12), channel_id=1, replica_groups=mesh['grp'=2,'ep'=4,'tp'=4] {'tp'}, use_global_device_ids=true, to_apply=%region_1.0 | all-reduce | flops 384 | bytes 3072 | tf_op jit(solution)/shard_map/psum | solution.py:17
  22.8 0.1 reshape.80
  22.9 0.7 dynamic_slice.3
  23.6 1.4 fusion.14
  24.9 1.0 gather_fusion
  26.0 0.1 broadcast_select_fusion
  26.1 10.5 %all_to_all.10 = bf16[4,48,1024]{2,1,0:T(8,128)(2,1)} all-to-all(bf16[4,48,1024]{2,1,0:T(8,128)(2,1)S(1)} %broadcast_select_fusion), channel_id=1, replica_groups=mesh['grp'=2,'ep'=4,'tp'=4] {'ep'}, dimensions={0} | all-to-all | bytes 786432 | tf_op jit(solution)/shard_map/all_to_all | solution.py:24
  36.5 0.0 all-gather.2.cloned.1.call-update
  36.6 0.0 reduce-scatter.2.cloned.1.call-start
  36.6 34.4 %all-gather.2.cloned.1.call-done = bf16[192,4096]{1,0:T(8,128)(2,1)} async-done(((bf16[192,1024]{1,0:T(8,128)(2,1)}), bf16[192,4096]{1,0:T(8,128)(2,1)}) %all-gather.2.cloned.1.call-update) | async-done | bytes 1572880 | tf_op jit(solution)/shard_map/all_gather | solution.py:25
  71.0 4.8 %fusion.4 = f32[192,768]{1,0:T(8,128)S(1)} fusion(bf16[192,4096]{1,0:T(8,128)(2,1)} %all-gather.2.cloned.1.call-done, bf16[1,4096,768]{2,1,0:T(8,128)(2,1)} %param.13), kind=kOutput, calls=%fused_computation.6 | convolution fusion | flops 1207959552 | bytes 8454144 | tf_op jit(solution)/shard_map/dot_general | solution.py:26
  75.8 9.3 %fusion.9 = bf16[4096,192]{0,1:T(8,128)(2,1)} fusion(bf16[1,768,4096]{2,1,0:T(8,128)(2,1)} %param.15, bf16[192,4096]{1,0:T(8,128)(2,1)S(1)} %copy-done.4, bf16[1,4096,768]{2,1,0:T(8,128)(2,1)} %param.14, f32[192,768]{1,0:T(8,128)S(1)} %fusion.4), kind=kOutput, calls=%fused_computation.9 | convolution fusion | flops 2417590272 | bytes 16318464 | tf_op jit(solution)/shard_map/dot_general | solution.py:31
  85.1 34.4 %reduce-scatter.2.cloned.1.call-done = bf16[1024,192]{0,1:T(8,128)(2,1)} async-done(((bf16[4096,192]{0,1:T(8,128)(2,1)}), bf16[1024,192]{0,1:T(8,128)(2,1)}) %reduce-scatter.2.cloned.1.call-update) | async-done | bytes 393232 | tf_op jit(solution)/shard_map/reduce_scatter | solution.py:30
  119.5 3.5 %all-to-all-start.1 = ((bf16[1024,4,48]{0,2,1:T(8,128)(2,1)}), bf16[1024,4,48]{0,2,1:T(8,128)(2,1)S(1)}, u32[]{:S(2)}, u32[]{:S(2)}) async-start(bf16[1024,4,48]{0,2,1:T(8,128)(2,1)} %bitcast.48), calls=%async_computation.2 | async-start | bytes 786432 | tf_op jit(solution)/shard_map/all_to_all | solution.py:39
  123.0 0.1 reshape_squeeze.3
  123.1 7.3 %all-to-all-done.1 = bf16[1024,4,48]{0,2,1:T(8,128)(2,1)S(1)} async-done(((bf16[1024,4,48]{0,2,1:T(8,128)(2,1)}), bf16[1024,4,48]{0,2,1:T(8,128)(2,1)S(1)}, u32[]{:S(2)}, u32[]{:S(2)}) %all-to-all-start.1) | async-done | bytes 393248 | tf_op jit(solution)/shard_map/all_to_all | solution.py:39
  130.3 0.1 convert_multiply_fusion.2
  130.5 2.5 %scatter_custom_fusion = f32[1024,384]{0,1:T(8,128)S(1)} fusion(s32[192]{0:T(256)S(1)} %bitcast.50, f32[192,1024]{1,0:T(8,128)S(1)} %bitcast.47, f32[]{:T(128)} %constant.11.clone.1), kind=kCustom, calls=%fused_computation.21 | custom fusion | flops 196608 | bytes 1572868 | tf_op jit(solution)/shard_map/scatter-add | solution.py:45
  133.0 0.3 multiply_reduce_fusion
  133.3 9.6 %psum.15 = f32[384]{0:T(512)S(1)} all-reduce(f32[384]{0:T(512)S(1)} %multiply_reduce_fusion), channel_id=1, replica_groups=mesh['grp'=2,'ep'=4,'tp'=4] {'tp'}, use_global_device_ids=true, to_apply=%region_5.6 | all-reduce | flops 384 | bytes 3072 | tf_op jit(solution)/shard_map/psum | solution.py:48
  142.9 1.1 multiply_convert_fusion
  (16 shorter events, 0.1 us)
Async XLA Ops:
  6.5 64.5 %all-gather.2.cloned.1.call-start = ((), (), s32[]{:S(2)}) async-start(), calls=%async_computation.3 | async-start | bytes 1966080 | tf_op jit(solution)/shard_map/all_gather | solution.py:25
  36.6 82.9 %reduce-scatter.2.cloned.1.call-start = ((), (), s32[]{:S(2)}) async-start(), calls=%async_computation.4 | async-start | bytes 1966080 | tf_op jit(solution)/shard_map/reduce_scatter | solution.py:30
  71.0 4.8 %copy-start.4 = (bf16[192,4096]{1,0:T(8,128)(2,1)S(1)}, bf16[192,4096]{1,0:T(8,128)(2,1)}, u32[]{:S(2)}) copy-start(bf16[192,4096]{1,0:T(8,128)(2,1)} %all-gather.2.cloned.1.call-done) | copy-start | bytes 4718596
  85.0 37.9 %copy-start.1 = (s32[1,4,48]{2,1,0:T(4,128)S(1)}, s32[1,4,48]{2,1,0:T(4,128)}, u32[]{:S(2)}) copy-start(s32[1,4,48]{2,1,0:T(4,128)} %param.11) | copy-start | bytes 2308
  85.0 45.3 %copy-start.3 = (f32[1,4,48]{2,1,0:T(4,128)S(1)}, f32[1,4,48]{2,1,0:T(4,128)}, u32[]{:S(2)}) copy-start(f32[1,4,48]{2,1,0:T(4,128)} %param.12) | copy-start | bytes 2308
  119.5 10.8 %all-to-all-start.1 = ((bf16[1024,4,48]{0,2,1:T(8,128)(2,1)}), bf16[1024,4,48]{0,2,1:T(8,128)(2,1)S(1)}, u32[]{:S(2)}, u32[]{:S(2)}) async-start(bf16[1024,4,48]{0,2,1:T(8,128)(2,1)} %bitcast.48), calls=%async_computation.2 | async-start | bytes 786432 | tf_op jit(solution)/shard_map/all_to_all | solution.py:39
  123.0 10.0 %copy-start = (bf16[384,1024]{1,0:T(8,128)(2,1)S(1)}, bf16[384,1024]{1,0:T(8,128)(2,1)}, u32[]{:S(2)}) copy-start(bf16[384,1024]{1,0:T(8,128)(2,1)} %param.8) | copy-start | bytes 2359300
  133.0 9.9 %copy-start.2 = (f32[1024]{0:T(1024)S(1)}, f32[1024]{0:T(1024)}, u32[]{:S(2)}) copy-start(f32[1024]{0:T(1024)} %param.10) | copy-start | bytes 12292
Sparse Core Ops, SparseCore 0:
  36.7 34.2 all-gather.1
  85.2 34.2 reduce-scatter.1
where the time goes:
time: 151 us
  waiting for transfers between devices  76.1 us (50%)
  blocking collectives  33.6 us (22%)
  matrix products  14 us (9%)
  between operations  13.5 us (9%)
  other arithmetic  8.29 us (5%)
  starting transfers between devices  3.5 us (2%)
  local copies, waits for them, and re-layouts  1.9 us (1%)
    reduce_scatter x1, waiting for transfers between devices, shards(): lax.psum_scatter(lax.dot_general(down_shard, hidden, (((0,), (1,)), ((),...  34.4 us
    all_gather x1, waiting for transfers between devices, shards(): lax.all_gather(incoming.reshape(-1, shard_width), 'tp', axis=1, tiled=True)  34.4 us
    psum x1, blocking collectives, shards(): square_sum = lax.psum(jnp.sum(resident * resident, axis=1), 'tp')  13.5 us
    all_to_all x1, blocking collectives, shards(): lax.all_to_all(outgoing, 'ep', split_axis=0, concat_axis=0, tiled=True)  10.5 us
    psum x1, blocking collectives, shards(): out_sum = lax.psum(jnp.sum(mixed_rows * mixed_rows, axis=1), 'tp')  9.64 us
    dot_general x1, matrix products, shards(): lax.dot_general(down_shard, hidden, (((0,), (1,)), ((), ())), preferred_e...  9.25 us
    all_to_all x1, waiting for transfers between devices, shards(): lax.all_to_all(expert_out, 'ep', split_axis=1, concat_axis=1, tiled=True)  7.26 us
    dot_general x1, matrix products, shards(): jnp.dot(picked_rows, expert_gate[0], preferred_element_type=jnp.float32)  4.76 us
  transfers between devices with their start and end apart: 3, of which 3 were waited for; matrix products, arithmetic and copies ran while one was open for 0% of the time, Pallas kernels for 0%

commit v1 on v0

--- a/solution.py
+++ b/solution.py
@@ -4,6 +4,27 @@
 from jax.sharding import PartitionSpec as P
 
 NORM_EPS = 1e-06
+
+
+def collect(shard, axis, dim):
+    length, position, rows = (lax.axis_size(axis), lax.axis_index(axis), shard.shape[dim])
+    right = [(i, (i + 1) % length) for i in range(length)]
+    left = [(i, (i - 1) % length) for i in range(length)]
+    result = jnp.zeros((*shard.shape[:dim], length * rows, *shard.shape[dim + 1 :]), shard.dtype)
+    result = lax.dynamic_update_slice_in_dim(result, shard, position * rows, axis=dim)
+    from_left = from_right = shard
+    middle = length // 2
+    for hop in range(1, middle + 1):
+        from_left = lax.ppermute(from_left, axis, right)
+        result = lax.dynamic_update_slice_in_dim(
+            result, from_left, (position - hop) % length * rows, axis=dim
+        )
+        if hop < length - middle:
+            from_right = lax.ppermute(from_right, axis, left)
+            result = lax.dynamic_update_slice_in_dim(
+                result, from_right, (position + hop) % length * rows, axis=dim
+            )
+    return result
 
 
 def shards(tokens, pre_gain, out_gain, chosen, route_weight, expert_gate, expert_up, expert_down):
@@ -22,7 +43,7 @@
     normed = (resident * row_scale * gain_slice).astype(jnp.bfloat16)
     outgoing = jnp.take(normed, chosen_here, axis=0)
     incoming = lax.all_to_all(outgoing, "ep", split_axis=0, concat_axis=0, tiled=True)
-    picked_rows = lax.all_gather(incoming.reshape(-1, shard_width), "tp", axis=1, tiled=True)
+    picked_rows = collect(incoming.reshape(-1, shard_width), "tp", 1)
     gate_act = jnp.dot(picked_rows, expert_gate[0], preferred_element_type=jnp.float32)
     up_act = jnp.dot(picked_rows, expert_up[0], preferred_element_type=jnp.float32)
     hidden = (jax.nn.silu(gate_act) * up_act).astype(jnp.bfloat16)

time: 151 us -> 144 us (0.954)
  waiting for transfers between devices: 76.1 us -> 65.5 us
  starting transfers between devices: 3.5 us -> 7.29 us
    all_gather x1 -> x0, waiting for transfers between devices: 34.4 us -> none  [shards(): lax.all_gather(incoming.reshape(-1, shard_width), 'tp', axis=1, tiled=True)]
    ppermute x0 -> x3, waiting for transfers between devices: none -> 25.1 us  [the longest x2 20.2 us: collect(): from_left = lax.ppermute(from_left, axis, right)]
    ppermute x0 -> x3, starting transfers between devices: none -> 3.83 us  [the longest x1 3.82 us: collect(): from_right = lax.ppermute(from_right, axis, left)]
  transfers between devices with their start and end apart: 3 -> 5, of which waited for: 3 -> 5; matrix products, arithmetic and copies ran while one was open for 0% -> 0% of each run, Pallas kernels for 0% -> 0%
where the time goes in v1:
time: 144 us; the launch traced here: 143 us
  waiting for transfers between devices  65.5 us (45%)
  blocking collectives  33.1 us (23%)
  between operations  13.5 us (9%)
  matrix products  13.4 us (9%)
  other arithmetic  8.29 us (6%)
  starting transfers between devices  7.29 us (5%)
  local copies, waits for them, and re-layouts  2.2 us (2%)
    reduce_scatter x1, waiting for transfers between devices, shards(): lax.psum_scatter(lax.dot_general(down_shard, hidden, (((0,), (1,)), ((),...  33.1 us
    ppermute x2, waiting for transfers between devices, collect(): from_left = lax.ppermute(from_left, axis, right)  20.2 us
    psum x1, blocking collectives, shards(): square_sum = lax.psum(jnp.sum(resident * resident, axis=1), 'tp')  13.5 us
    all_to_all x1, blocking collectives, shards(): lax.all_to_all(outgoing, 'ep', split_axis=0, concat_axis=0, tiled=True)  10 us
    psum x1, blocking collectives, shards(): out_sum = lax.psum(jnp.sum(mixed_rows * mixed_rows, axis=1), 'tp')  9.64 us
    dot_general x1, matrix products, shards(): lax.dot_general(down_shard, hidden, (((0,), (1,)), ((), ())), preferred_e...  9.26 us
    all_to_all x1, waiting for transfers between devices, shards(): lax.all_to_all(expert_out, 'ep', split_axis=1, concat_axis=1, tiled=True)  7.26 us
    ppermute x1, waiting for transfers between devices, collect(): from_right = lax.ppermute(from_right, axis, left)  4.87 us
  transfers between devices with their start and end apart: 5, of which 5 were waited for; matrix products, arithmetic and copies ran while one was open for 0% of the time, Pallas kernels for 0%

profile of v1, /device:TPU:0, one launch (start us, length us, event | category | flops | bytes accessed | tf_op | source)
XLA Modules:
  0.0 143.3 jit_solution(15904103290121605581)
XLA Ops:
  6.5 0.7 compare_select_fusion.1
  7.2 0.7 compare_and_fusion
  7.9 1.4 fusion.12
  9.3 13.5 %psum.14 = f32[384]{0:T(512)S(1)} all-reduce(f32[384]{0:T(512)S(1)} %fusion.12), channel_id=1, replica_groups=mesh['grp'=2,'ep'=4,'tp'=4] {'tp'}, use_global_device_ids=true, to_apply=%region_1.0 | all-reduce | flops 384 | bytes 3072 | tf_op jit(solution)/shard_map/psum | solution.py:38
  22.9 0.7 dynamic_slice.3
  23.6 1.4 fusion.14
  24.9 1.0 gather_fusion
  26.0 0.1 broadcast_select_fusion
  26.1 10.0 %all_to_all.10 = bf16[4,48,1024]{2,1,0:T(8,128)(2,1)S(1)} all-to-all(bf16[4,48,1024]{2,1,0:T(8,128)(2,1)S(1)} %broadcast_select_fusion), channel_id=1, replica_groups=mesh['grp'=2,'ep'=4,'tp'=4] {'ep'}, dimensions={0} | all-to-all | bytes 786432 | tf_op jit(solution)/shard_map/all_to_all | solution.py:45
  36.1 3.8 %collective-permute-start.1 = (bf16[192,1024]{1,0:T(8,128)(2,1)S(1)}, bf16[192,1024]{1,0:T(8,128)(2,1)S(1)}, u32[]{:S(2)}, u32[]{:S(2)}) collective-permute-start(bf16[192,1024]{1,0:T(8,128)(2,1)S(1)} %bitcast.45), channel_id=1, source_target_pairs={{0,3},{1,0},{2,1},{3,2},{4,7},{5,4},{6,5},{7,6},{8,11},{9,8},{10,9... | collective-permute-start | bytes 1179656 | tf_op jit(solution)/shard_map/ppermute | solution.py:23
  39.9 10.0 %collective-permute-done = bf16[192,1024]{1,0:T(8,128)(2,1)S(1)} collective-permute-done((bf16[192,1024]{1,0:T(8,128)(2,1)S(1)}, bf16[192,1024]{1,0:T(8,128)(2,1)S(1)}, u32[]{:S(2)}, u32[]{:S(2)}) %collective-permute-start) | collective-permute-done | bytes 393248 | tf_op jit(solution)/shard_map/ppermute | solution.py:18
  49.9 0.2 broadcast_in_dim.22
  50.1 4.9 %collective-permute-done.1 = bf16[192,1024]{1,0:T(8,128)(2,1)S(1)} collective-permute-done((bf16[192,1024]{1,0:T(8,128)(2,1)S(1)}, bf16[192,1024]{1,0:T(8,128)(2,1)S(1)}, u32[]{:S(2)}, u32[]{:S(2)}) %collective-permute-start.1) | collective-permute-done | bytes 393248 | tf_op jit(solution)/shard_map/ppermute | solution.py:23
  55.0 10.2 %collective-permute-done.2 = bf16[192,1024]{1,0:T(8,128)(2,1)S(1)} collective-permute-done((bf16[192,1024]{1,0:T(8,128)(2,1)S(1)}, bf16[192,1024]{1,0:T(8,128)(2,1)S(1)}, u32[]{:S(2)}, u32[]{:S(2)}) %collective-permute-start.2) | collective-permute-done | bytes 393248 | tf_op jit(solution)/shard_map/ppermute | solution.py:18
  65.3 4.2 %fusion.2 = f32[192,768]{1,0:T(8,128)S(1)} fusion(bf16[192,4096]{1,0:T(8,128)(2,1)S(1)} %constant_dynamic-update-slice_fusion, bf16[1,4096,768]{2,1,0:T(8,128)(2,1)} %param.14), kind=kOutput, calls=%fused_computation.4 | convolution fusion | flops 1207959552 | bytes 8454144 | tf_op jit(solution)/shard_map/dot_general | solution.py:48
  69.5 9.3 %fusion.9 = bf16[4096,192]{0,1:T(8,128)(2,1)} fusion(bf16[1,768,4096]{2,1,0:T(8,128)(2,1)} %param.15, f32[192,768]{1,0:T(8,128)S(1)} %fusion.2, bf16[192,4096]{1,0:T(8,128)(2,1)S(1)} %constant_dynamic-update-slice_fusion, bf16[1,4096,768]{2,1,0:T(8,128)(2,1)} %param.13), kind=kOutput, calls=%fused_computation.9 | convolution fusion | flops 2417590272 | bytes 16318464 | tf_op jit(solution)/shard_map/dot_general | solution.py:52
  78.8 33.1 %reduce-scatter.2.cloned.1.call-done = bf16[1024,192]{0,1:T(8,128)(2,1)} async-done(((bf16[4096,192]{0,1:T(8,128)(2,1)}), bf16[1024,192]{0,1:T(8,128)(2,1)}) %reduce-scatter.2.cloned.1.call-update) | async-done | bytes 393232 | tf_op jit(solution)/shard_map/reduce_scatter | solution.py:51
  111.9 3.5 %all-to-all-start.1 = ((bf16[1024,4,48]{0,2,1:T(8,128)(2,1)}), bf16[1024,4,48]{0,2,1:T(8,128)(2,1)S(1)}, u32[]{:S(2)}, u32[]{:S(2)}) async-start(bf16[1024,4,48]{0,2,1:T(8,128)(2,1)} %bitcast.48), calls=%async_computation.2 | async-start | bytes 786432 | tf_op jit(solution)/shard_map/all_to_all | solution.py:60
  115.5 7.3 %all-to-all-done.1 = bf16[1024,4,48]{0,2,1:T(8,128)(2,1)S(1)} async-done(((bf16[1024,4,48]{0,2,1:T(8,128)(2,1)}), bf16[1024,4,48]{0,2,1:T(8,128)(2,1)S(1)}, u32[]{:S(2)}, u32[]{:S(2)}) %all-to-all-start.1) | async-done | bytes 393248 | tf_op jit(solution)/shard_map/all_to_all | solution.py:60
  122.7 0.1 convert_multiply_fusion.2
  122.9 2.5 %scatter_custom_fusion = f32[1024,384]{0,1:T(8,128)S(1)} fusion(s32[192]{0:T(256)S(1)} %bitcast.50, f32[192,1024]{1,0:T(8,128)S(1)} %bitcast.47, f32[]{:T(128)} %constant.51.clone.1), kind=kCustom, calls=%fused_computation.19 | custom fusion | flops 196608 | bytes 1572868 | tf_op jit(solution)/shard_map/scatter-add | solution.py:66
  125.4 0.3 multiply_reduce_fusion
  125.7 9.6 %psum.15 = f32[384]{0:T(512)S(1)} all-reduce(f32[384]{0:T(512)S(1)} %multiply_reduce_fusion), channel_id=1, replica_groups=mesh['grp'=2,'ep'=4,'tp'=4] {'tp'}, use_global_device_ids=true, to_apply=%region_5.6 | all-reduce | flops 384 | bytes 3072 | tf_op jit(solution)/shard_map/psum | solution.py:69
  135.3 1.1 multiply_convert_fusion
  (22 shorter events, 0.4 us)
Async XLA Ops:
  6.5 105.4 %reduce-scatter.2.cloned.1.call-start = ((), (), s32[]{:S(2)}) async-start(), calls=%async_computation.3 | async-start | bytes 1966080 | tf_op jit(solution)/shard_map/reduce_scatter | solution.py:51
  36.1 13.8 %collective-permute-start = (bf16[192,1024]{1,0:T(8,128)(2,1)S(1)}, bf16[192,1024]{1,0:T(8,128)(2,1)S(1)}, u32[]{:S(2)}, u32[]{:S(2)}) collective-permute-start(bf16[192,1024]{1,0:T(8,128)(2,1)S(1)} %bitcast.44), channel_id=1, source_target_pairs={{0,1},{1,2},{2,3},{3,0},{4,5},{5,6},{6,7},{7,4},{8,9},{9,10},{10,1... | collective-permute-start | bytes 1179656 | tf_op jit(solution)/shard_map/ppermute | solution.py:18
  36.1 18.9 %collective-permute-start.1 = (bf16[192,1024]{1,0:T(8,128)(2,1)S(1)}, bf16[192,1024]{1,0:T(8,128)(2,1)S(1)}, u32[]{:S(2)}, u32[]{:S(2)}) collective-permute-start(bf16[192,1024]{1,0:T(8,128)(2,1)S(1)} %bitcast.45), channel_id=1, source_target_pairs={{0,3},{1,0},{2,1},{3,2},{4,7},{5,4},{6,5},{7,6},{8,11},{9,8},{10,9... | collective-permute-start | bytes 1179656 | tf_op jit(solution)/shard_map/ppermute | solution.py:23
  49.8 15.4 %collective-permute-start.2 = (bf16[192,1024]{1,0:T(8,128)(2,1)S(1)}, bf16[192,1024]{1,0:T(8,128)(2,1)S(1)}, u32[]{:S(2)}, u32[]{:S(2)}) collective-permute-start(bf16[192,1024]{1,0:T(8,128)(2,1)S(1)} %collective-permute-done), channel_id=1, source_target_pairs={{0,1},{1,2},{2,3},{3,0},{4,5},{5,6},{6,7},{7,4},{8,9},{9,10},{10,1... | collective-permute-start | bytes 1179656 | tf_op jit(solution)/shard_map/ppermute | solution.py:18
  78.7 36.6 %copy-start.1 = (s32[1,4,48]{2,1,0:T(4,128)S(1)}, s32[1,4,48]{2,1,0:T(4,128)}, u32[]{:S(2)}) copy-start(s32[1,4,48]{2,1,0:T(4,128)} %param.11) | copy-start | bytes 2308
  78.7 44.0 %copy-start.3 = (f32[1,4,48]{2,1,0:T(4,128)S(1)}, f32[1,4,48]{2,1,0:T(4,128)}, u32[]{:S(2)}) copy-start(f32[1,4,48]{2,1,0:T(4,128)} %param.12) | copy-start | bytes 2308
  111.9 10.8 %all-to-all-start.1 = ((bf16[1024,4,48]{0,2,1:T(8,128)(2,1)}), bf16[1024,4,48]{0,2,1:T(8,128)(2,1)S(1)}, u32[]{:S(2)}, u32[]{:S(2)}) async-start(bf16[1024,4,48]{0,2,1:T(8,128)(2,1)} %bitcast.48), calls=%async_computation.2 | async-start | bytes 786432 | tf_op jit(solution)/shard_map/all_to_all | solution.py:60
  115.4 10.0 %copy-start = (bf16[384,1024]{1,0:T(8,128)(2,1)S(1)}, bf16[384,1024]{1,0:T(8,128)(2,1)}, u32[]{:S(2)}) copy-start(bf16[384,1024]{1,0:T(8,128)(2,1)} %param.8) | copy-start | bytes 2359300
  125.4 9.9 %copy-start.2 = (f32[1024]{0:T(1024)S(1)}, f32[1024]{0:T(1024)}, u32[]{:S(2)}) copy-start(f32[1024]{0:T(1024)} %param.10) | copy-start | bytes 12292
Sparse Core Ops, SparseCore 0:
  78.9 32.9 reduce-scatter.1
